TPU v7x, 32 devices: a whole 2x2x4 slice. The times are simulated.
32 devices in a mesh: sp: 4 (over z), tp: 4 (over y, x), dp: 2 (over core).
Axes of the slice: x: 2, y: 2, z: 4, core: 2. Of those that a mesh axis runs over, the one named last changes fastest.
Arguments:
- latent: bfloat16 [4, 4096, 2048], P('dp', 'sp'), may hold values from -6 to 6
- context: bfloat16 [4, 1024, 2048], P('dp', 'sp'), may hold values from -6 to 6
- condition: bfloat16 [4, 2048], P('dp', 'sp'), may hold values from -6 to 6
- ctx_cond: bfloat16 [2048], P('sp'), may hold values from -6 to 6
- norm_gain: float32 [2048], replicated, may hold values from 0.1 to 1.9
- w_shift: bfloat16 [2048, 2048], P('sp', 'tp'), may hold values from -0.125 to 0.125
- w_scale: bfloat16 [2048, 2048], P('sp', 'tp'), may hold values from -0.125 to 0.125
- w_gate: bfloat16 [2048, 2048], P('sp', 'tp'), may hold values from -0.125 to 0.125
- w_query: bfloat16 [2048, 1024], P(None, 'tp'), may hold values from -0.125 to 0.125
- w_key: bfloat16 [2048, 256], P(None, 'tp'), may hold values from -0.125 to 0.125
- w_value: bfloat16 [2048, 256], P(None, 'tp'), may hold values from -0.125 to 0.125
- w_out: bfloat16 [1024, 2048], P('tp'), may hold values from -4 to 4
- sink_logit: float32 [16], P('tp'), may hold values from 4 to 7
- ctx_lift: float32 [16], P('tp'), may hold values from -4 to 220
Outputs:
- mixed: bfloat16 [4, 4096, 2048], P('dp', ('sp', 'tp'))
All inputs are finite; a program needn't handle non-finite values.
Results may differ from a plain program's by a relative error of at most 0.012.
Values may be sent and summed in bfloat16 or wider, within the bound.
A program may use at most 128 MiB of HBM per device.

v0:
```python
import functools
import math

import jax
import jax.numpy as jnp
from jax import lax
from jax.experimental import pallas as pl
from jax.experimental.pallas import tpu as pltpu
from jax.sharding import PartitionSpec as P

HEAD = 64
WINDOW = 128
GRID_COLS = 64
LANES = 128

epsilon = 1e-06
rope_base = 10000.0
masked_value = -1e30
log2e = 1.4426950408889634
MESH = pl.DeviceIdType.MESH


def kernel(
    sizes,
    latent,
    context,
    condition,
    ctx_cond,
    norm_gain,
    w_shift,
    w_scale,
    w_gate,
    w_query,
    w_key,
    w_value,
    w_out,
    sink_logit,
    ctx_lift,
    out,
    x_lat,
    x_ctx,
    w_mod,
    w_q,
    w_kvt,
    w_kv,
    cos_tab,
    sin_tab,
    w_o,
    act,
    mod_rx,
    mod_all,
    vec_a,
    vec_b,
    vec_g,
    inv_lat,
    inv_ctx,
    q_buf,
    kv_buf,
    v_buf,
    ckv_buf,
    cv_buf,
    mask_buf,
    att_buf,
    rows_rx,
    ld_sem,
    ma_send,
    ma_recv,
    mb_send,
    mb_recv,
    cx_send,
    cx_recv,
    ha_send,
    ha_recv,
    at_send,
    at_recv,
    wo_send,
    wo_recv,
    wf_send,
    wf_recv,
):
    n_sp, n_tp, n_dp = sizes
    me_sp, me_tp, me_dp = lax.axis_index("sp"), lax.axis_index("tp"), lax.axis_index("dp")
    samples, tokens, width = latent.shape
    ctx_rows = context.shape[1]
    part = w_shift.shape[1]
    heads = w_query.shape[1] // HEAD
    block = tokens // n_tp
    span = block + 2 * WINDOW

    def other(me, step, count):
        return lax.rem(me + step, count)

    barrier = pltpu.get_barrier_semaphore()
    for axis, me, count in (("sp", me_sp, n_sp), ("tp", me_tp, n_tp), ("dp", me_dp, n_dp)):
        for step in range(1, count):
            pl.semaphore_signal(
                barrier, inc=1, device_id={axis: other(me, step, count)}, device_id_type=MESH
            )

    loads = []
    for source, target in (
        (w_shift, w_mod.at[0]),
        (w_scale, w_mod.at[1]),
        (w_gate, w_mod.at[2]),
        (context, x_ctx),
        (latent.at[0], x_lat.at[0]),
        (w_key, w_kvt.at[0:HEAD]),
        (w_value, w_kvt.at[HEAD : 2 * HEAD]),
        (w_query, w_q),
        *((latent.at[s], x_lat.at[s]) for s in range(1, samples)),
        (w_out, w_o.at[me_tp]),
    ):
        copy = pltpu.make_async_copy(source, target, ld_sem.at[len(loads)])
        copy.start()
        loads.append(copy)

    act[...] = jnp.zeros_like(act)
    cond = condition[...].astype(jnp.float32)
    act[0:samples, :] = cond / (1.0 + jnp.exp(-cond))
    cond = ctx_cond[...].astype(jnp.float32).reshape(1, -1)
    act[samples : samples + 1, :] = cond / (1.0 + jnp.exp(-cond))
    active = act[...].astype(jnp.bfloat16)
    for i in range(3):
        loads[i].wait()
        mod_rx[me_sp, :, i * part : (i + 1) * part] = jnp.dot(
            active, w_mod[i], preferred_element_type=jnp.float32
        )
    pl.semaphore_wait(barrier, n_sp + n_tp + n_dp - 3)

    def mod_copy(step):
        return pltpu.make_async_remote_copy(
            src_ref=mod_rx.at[me_sp],
            dst_ref=mod_rx.at[me_sp],
            send_sem=ma_send.at[step],
            recv_sem=ma_recv.at[step],
            device_id={"sp": other(me_sp, step, n_sp)},
            device_id_type=MESH,
        )

    for step in range(1, n_sp):
        mod_copy(step).start()

    def inverse_of(rows):
        wide = rows.astype(jnp.float32)
        total = jnp.sum(wide * wide, axis=-1, keepdims=True)
        return jnp.broadcast_to(lax.rsqrt(total / width + epsilon), (rows.shape[0], LANES))

    loads[3].wait()
    for s in range(samples):
        inv_ctx[s] = inverse_of(x_ctx[s])

    def stats(s):
        def body(i, carry):
            rows = pl.ds(pl.multiple_of(i * block, block), block)
            inv_lat[s, rows, :] = inverse_of(x_lat[s, rows, :])
            return carry

        lax.fori_loop(0, n_tp, body, 0)

    loads[4].wait()
    stats(0)
    loads[5].wait()
    loads[6].wait()
    w_kv[...] = w_kvt[...].T
    fill_tables(me_sp * (tokens // GRID_COLS), cos_tab, sin_tab)

    def wait_mod(step):
        source = other(me_sp, n_sp - step, n_sp)
        pltpu.make_async_remote_copy(
            src_ref=mod_rx.at[source],
            dst_ref=mod_rx.at[source],
            send_sem=ma_send.at[step],
            recv_sem=ma_recv.at[step],
            device_id={"sp": other(me_sp, step, n_sp)},
            device_id_type=MESH,
        ).wait_recv()

    for step in range(1, n_sp):
        wait_mod(step)
    total = mod_rx[0]
    for i in range(1, n_sp):
        total = total + mod_rx[i]
    mod_all[me_tp] = total

    def all_copy(step, source):
        return pltpu.make_async_remote_copy(
            src_ref=mod_all.at[source],
            dst_ref=mod_all.at[source],
            send_sem=mb_send.at[step],
            recv_sem=mb_recv.at[step],
            device_id={"tp": other(me_tp, step, n_tp)},
            device_id_type=MESH,
        )

    for step in range(1, n_tp):
        all_copy(step, me_tp).start()
    for s in range(1, samples):
        loads[7 + s].wait()
        stats(s)
    loads[7].wait()
    for step in range(1, n_tp):
        all_copy(step, other(me_tp, n_tp - step, n_tp)).wait_recv()
    for t in range(n_tp):
        cols = slice(t * part, (t + 1) * part)
        vec_b[:, cols] = mod_all[t, :, 0:part]
        vec_a[:, cols] = (1.0 + mod_all[t, :, part : 2 * part]) * norm_gain[:, cols]
        vec_g[:, cols] = mod_all[t, :, 2 * part : 3 * part]

    share = w_out.shape[0] // n_dp
    mine = pl.ds(pl.multiple_of(me_dp * share, share), share)

    def out_copy(step, source):
        return pltpu.make_async_remote_copy(
            src_ref=w_out.at[mine, :],
            dst_ref=w_o.at[source, mine, :],
            send_sem=wo_send.at[step],
            recv_sem=wo_recv.at[step],
            device_id={"tp": other(me_tp, step, n_tp)},
            device_id_type=MESH,
        )

    def forward_copy(step, hop, part_id):
        source = other(me_tp, n_tp - step, n_tp)
        rows = pl.ds(pl.multiple_of(part_id * share, share), share)
        return pltpu.make_async_remote_copy(
            src_ref=w_o.at[source, rows, :],
            dst_ref=w_o.at[source, rows, :],
            send_sem=wf_send.at[step, hop],
            recv_sem=wf_recv.at[step, hop],
            device_id={"dp": other(me_dp, hop, n_dp)},
            device_id_type=MESH,
        )

    for step in range(1, n_tp):
        out_copy(step, me_tp).start()

    def hidden_of(rows, inverse, row):
        return (
            rows.astype(jnp.float32) * inverse[:, 0:1] * vec_a[row : row + 1, :]
            + vec_b[row : row + 1, :]
        ).astype(jnp.bfloat16)

    def ctx_copy(s, step, source):
        rows = pl.ds(pl.multiple_of(source * ctx_rows, ctx_rows), ctx_rows)
        return pltpu.make_async_remote_copy(
            src_ref=ckv_buf.at[s, rows, :],
            dst_ref=ckv_buf.at[s, rows, :],
            send_sem=cx_send.at[s, step],
            recv_sem=cx_recv.at[s, step],
            device_id={"sp": other(me_sp, step, n_sp)},
            device_id_type=MESH,
        )

    for s in range(samples):
        rows = pl.ds(pl.multiple_of(me_sp * ctx_rows, ctx_rows), ctx_rows)
        ckv_buf[s, rows, :] = jnp.dot(
            hidden_of(x_ctx[s], inv_ctx[s], samples), w_kv[...], preferred_element_type=jnp.float32
        ).astype(jnp.bfloat16)
        for step in range(1, n_sp):
            ctx_copy(s, step, me_sp).start()

    lane = lax.broadcasted_iota(jnp.int32, (block, LANES), 1)
    quarter = HEAD // 4
    first = lane % (2 * quarter) < quarter
    low = lane < HEAD

    def turned(u, cos_rows, sin_rows):
        partner = jnp.where(
            first, pltpu.roll(u, LANES - quarter, 1), pltpu.roll(u, quarter, 1)
        )
        return u * cos_rows + partner * sin_rows

    def project(s):
        def body(i, carry):
            start = pl.multiple_of(i * block, block)
            rows = pl.ds(start, block)
            hid = hidden_of(x_lat[s, rows, :], inv_lat[s, rows, :], s)
            cos_rows, sin_rows = cos_tab[rows, :], sin_tab[rows, :]
            kv = jnp.dot(hid, w_kv[...], preferred_element_type=jnp.float32)
            kv = jnp.where(low, turned(kv, cos_rows, sin_rows), kv)
            kv_buf[s, pl.ds(pl.multiple_of(start + WINDOW, WINDOW), block), :] = kv.astype(
                jnp.bfloat16
            )
            q = jnp.dot(hid, w_q[...], preferred_element_type=jnp.float32)
            scale = log2e * HEAD ** (-0.5)
            for pair in range(heads // 2):
                u = turned(q[:, pair * LANES : (pair + 1) * LANES], cos_rows, sin_rows) * scale
                q_buf[s, 2 * pair, rows, :] = jnp.where(low, u, 0.0).astype(jnp.bfloat16)
                q_buf[s, 2 * pair + 1, rows, :] = jnp.where(
                    low, pltpu.roll(u, HEAD, 1), 0.0
                ).astype(jnp.bfloat16)
            return carry

        lax.fori_loop(0, n_tp, body, 0)

    def halo_copy(s, side):
        source, target = ((tokens, 0), (WINDOW, WINDOW + tokens))[side]
        step = (1, n_sp - 1)[side]
        return pltpu.make_async_remote_copy(
            src_ref=kv_buf.at[s, pl.ds(source, WINDOW), :],
            dst_ref=kv_buf.at[s, pl.ds(target, WINDOW), :],
            send_sem=ha_send.at[s, side],
            recv_sem=ha_recv.at[s, side],
            device_id={"sp": other(me_sp, step, n_sp)},
            device_id_type=MESH,
        )

    for s in range(samples):
        project(s)
        halo_copy(s, 0).start()
        halo_copy(s, 1).start()

    for s in range(samples):
        for step in range(1, n_sp):
            ctx_copy(s, step, other(me_sp, n_sp - step, n_sp)).wait_recv()
        rows = ckv_buf[s]
        keep = lax.broadcasted_iota(jnp.int32, rows.shape, 1) >= HEAD
        cv_buf[s] = jnp.where(keep, rows.astype(jnp.float32), 1.0).astype(jnp.bfloat16)
    for s in range(samples):
        for side in range(2):
            halo_copy(s, side).wait_recv()
        rows = kv_buf[s]
        keep = lax.broadcasted_iota(jnp.int32, rows.shape, 1) >= HEAD
        v_buf[s] = jnp.where(keep, rows.astype(jnp.float32), 1.0).astype(jnp.bfloat16)

    def rows_copy(s, step, source):
        target = other(me_tp, step, n_tp)
        return pltpu.make_async_remote_copy(
            src_ref=att_buf.at[s, target],
            dst_ref=rows_rx.at[source, s],
            send_sem=at_send.at[s, step],
            recv_sem=at_recv.at[s, step],
            device_id={"tp": target},
            device_id_type=MESH,
        )

    nt = (((1,), (1,)), ((), ()))
    row_id = lax.broadcasted_iota(jnp.int32, (block, span), 0)
    col_id = lax.broadcasted_iota(jnp.int32, (block, span), 1)

    def attend(index, carry):
        s = index // n_tp
        step = index % n_tp + 1
        owner = other(me_tp, step, n_tp)
        start = pl.multiple_of(owner * block, block)
        key_pos = me_sp * tokens + start - WINDOW + col_id
        inside = (
            (key_pos >= 0)
            & (key_pos < n_sp * tokens)
            & (jnp.abs(row_id + WINDOW - col_id) <= WINDOW)
        )
        mask_buf[...] = jnp.where(inside, 0.0, masked_value)
        for h in range(heads):
            q = q_buf[s, h, pl.ds(start, block), :]
            far = lax.dot_general(q, ckv_buf[s], nt, preferred_element_type=jnp.float32)
            near = (
                lax.dot_general(
                    q, kv_buf[s, pl.ds(start, span), :], nt, preferred_element_type=jnp.float32
                )
                + mask_buf[...]
            )
            lift = ctx_lift[h] * log2e
            sink = sink_logit[h] * log2e
            top = jnp.maximum(
                jnp.maximum(
                    jnp.max(near, axis=-1, keepdims=True),
                    jnp.max(far, axis=-1, keepdims=True) + lift,
                ),
                sink,
            )
            near_exp = jnp.exp2(near - top).astype(jnp.bfloat16)
            far_exp = jnp.exp2(far - (top - lift)).astype(jnp.bfloat16)
            both = jnp.dot(
                near_exp, v_buf[s, pl.ds(start, span), :], preferred_element_type=jnp.float32
            ) + jnp.dot(far_exp, cv_buf[s], preferred_element_type=jnp.float32)
            weight = both[:, 0:HEAD] + jnp.exp2(sink - top)
            att_buf[s, owner, :, h * HEAD : (h + 1) * HEAD] = (both[:, HEAD:] / weight).astype(
                jnp.bfloat16
            )

        @pl.when(step < n_tp)
        def _():
            rows_copy(s, step, me_tp).start()

        @pl.when(step == n_tp)
        def _():
            rows_rx[me_tp, s] = att_buf[s, me_tp]

        @pl.when(index == n_tp)
        def _():
            for hop_step in range(1, n_tp):
                out_copy(hop_step, other(me_tp, n_tp - hop_step, n_tp)).wait_recv()
                for hop in range(1, n_dp):
                    forward_copy(hop_step, hop, me_dp).start()

        return carry

    lax.fori_loop(0, samples * n_tp, attend, 0)

    loads[8 + samples - 1].wait()
    for step in range(1, n_tp):
        for hop in range(1, n_dp):
            forward_copy(step, hop, other(me_dp, n_dp - hop, n_dp)).wait_recv()
    chunk = 512
    for s in range(samples):
        for step in range(1, n_tp):
            rows_copy(s, step, other(me_tp, n_tp - step, n_tp)).wait_recv()

        def finish(i, carry):
            cols = pl.ds(pl.multiple_of(i * chunk, chunk), chunk)
            acc = jnp.dot(rows_rx[0, s], w_o[0, :, cols], preferred_element_type=jnp.float32)
            for t in range(1, n_tp):
                acc += jnp.dot(rows_rx[t, s], w_o[t, :, cols], preferred_element_type=jnp.float32)
            out[s, :, cols] = (acc * vec_g[s : s + 1, cols]).astype(jnp.bfloat16)
            return carry

        lax.fori_loop(0, width // chunk, finish, 0)

    for step in range(1, n_sp):
        mod_copy(step).wait_send()
        for s in range(samples):
            ctx_copy(s, step, me_sp).wait_send()
    for s in range(samples):
        halo_copy(s, 0).wait_send()
        halo_copy(s, 1).wait_send()
    for step in range(1, n_tp):
        all_copy(step, me_tp).wait_send()
        out_copy(step, me_tp).wait_send()
        for hop in range(1, n_dp):
            forward_copy(step, hop, me_dp).wait_send()
        for s in range(samples):
            rows_copy(s, step, me_tp).wait_send()


def fill_tables(first_row, cos_tab, sin_tab):
    tokens = cos_tab.shape[0]
    count = tokens // GRID_COLS
    quarter = HEAD // 4

    def angles_of(ticks, lane):
        power = (lane % quarter).astype(jnp.float32) * (-math.log(rope_base) / quarter)
        return ticks.astype(jnp.float32) * jnp.exp(power)

    def pair(ticks, lane):
        angles = angles_of(ticks, lane)
        sign = jnp.where(lane % (2 * quarter) < quarter, -1.0, 1.0)
        return jnp.cos(angles), jnp.sin(angles) * sign

    shape = (GRID_COLS, LANES)
    lane = lax.broadcasted_iota(jnp.int32, shape, 1)
    cos_col, sin_col = pair(lax.broadcasted_iota(jnp.int32, shape, 0), lane)
    by_row = lane % HEAD < HEAD // 2
    lines = (count, LANES)
    lane = lax.broadcasted_iota(jnp.int32, lines, 1)
    cos_row, sin_row = pair(lax.broadcasted_iota(jnp.int32, lines, 0) + first_row, lane)
    for r in range(count):
        rows = slice(r * GRID_COLS, (r + 1) * GRID_COLS)
        cos_tab[rows, :] = jnp.where(by_row, cos_row[r : r + 1, :], cos_col)
        sin_tab[rows, :] = jnp.where(by_row, sin_row[r : r + 1, :], sin_col)


def shards(
    latent,
    context,
    condition,
    ctx_cond,
    norm_gain,
    w_shift,
    w_scale,
    w_gate,
    w_query,
    w_key,
    w_value,
    w_out,
    sink_logit,
    ctx_lift,
):
    samples, tokens, width = latent.shape
    ctx_rows = context.shape[1]
    n_sp, n_tp, n_dp = lax.axis_size("sp"), lax.axis_size("tp"), lax.axis_size("dp")
    heads = w_query.shape[1] // HEAD
    assert w_key.shape[1] == HEAD and tokens % GRID_COLS == 0 and samples < 8 and heads % 2 == 0
    part = w_shift.shape[1]
    block = tokens // n_tp
    bf16, f32 = jnp.bfloat16, jnp.float32
    vmem = pl.BlockSpec(memory_space=pltpu.VMEM)
    smem = pl.BlockSpec(memory_space=pltpu.SMEM)
    anywhere = pl.BlockSpec(memory_space=pl.ANY)
    dma = pltpu.SemaphoreType.DMA
    padded = tokens + 2 * WINDOW
    return pl.pallas_call(
        functools.partial(kernel, (n_sp, n_tp, n_dp)),
        out_shape=jax.ShapeDtypeStruct((samples, block, width), bf16),
        in_specs=[
            anywhere,
            anywhere,
            vmem,
            vmem,
            vmem,
            anywhere,
            anywhere,
            anywhere,
            anywhere,
            anywhere,
            anywhere,
            anywhere,
            smem,
            smem,
        ],
        out_specs=vmem,
        scratch_shapes=[
            pltpu.VMEM(latent.shape, bf16),
            pltpu.VMEM(context.shape, bf16),
            pltpu.VMEM((3,) + w_shift.shape, bf16),
            pltpu.VMEM(w_query.shape, bf16),
            pltpu.VMEM((2 * HEAD, width), bf16),
            pltpu.VMEM((width, 2 * HEAD), bf16),
            pltpu.VMEM((tokens, LANES), f32),
            pltpu.VMEM((tokens, LANES), f32),
            pltpu.VMEM((n_tp,) + w_out.shape, bf16),
            pltpu.VMEM((8, w_shift.shape[0]), f32),
            pltpu.VMEM((n_sp, 8, 3 * part), f32),
            pltpu.VMEM((n_tp, 8, 3 * part), f32),
            pltpu.VMEM((8, width), f32),
            pltpu.VMEM((8, width), f32),
            pltpu.VMEM((8, width), f32),
            pltpu.VMEM((samples, tokens, LANES), f32),
            pltpu.VMEM((samples, ctx_rows, LANES), f32),
            pltpu.VMEM((samples, heads, tokens, LANES), bf16),
            pltpu.VMEM((samples, padded, LANES), bf16),
            pltpu.VMEM((samples, padded, LANES), bf16),
            pltpu.VMEM((samples, n_sp * ctx_rows, LANES), bf16),
            pltpu.VMEM((samples, n_sp * ctx_rows, LANES), bf16),
            pltpu.VMEM((block, block + 2 * WINDOW), f32),
            pltpu.VMEM((samples, n_tp, block, heads * HEAD), bf16),
            pltpu.VMEM((n_tp, samples, block, heads * HEAD), bf16),
            dma((8 + samples,)),
            dma((n_sp,)),
            dma((n_sp,)),
            dma((n_tp,)),
            dma((n_tp,)),
            dma((samples, n_sp)),
            dma((samples, n_sp)),
            dma((samples, 2)),
            dma((samples, 2)),
            dma((samples, n_tp)),
            dma((samples, n_tp)),
            dma((n_tp,)),
            dma((n_tp,)),
            dma((n_tp, n_dp)),
            dma((n_tp, n_dp)),
        ],
        compiler_params=pltpu.CompilerParams(
            collective_id=0, has_side_effects=True, vmem_limit_bytes=60 * 1024 * 1024
        ),
    )(
        latent,
        context,
        condition,
        ctx_cond,
        norm_gain.reshape(1, -1),
        w_shift,
        w_scale,
        w_gate,
        w_query,
        w_key.T,
        w_value.T,
        w_out,
        sink_logit,
        ctx_lift,
    )


def solution(mesh):
    return jax.shard_map(
        shards,
        mesh=mesh,
        in_specs=(
            P("dp", "sp", None),
            P("dp", "sp", None),
            P("dp", "sp"),
            P("sp"),
            P(),
            P("sp", "tp"),
            P("sp", "tp"),
            P("sp", "tp"),
            P(None, "tp"),
            P(None, "tp"),
            P(None, "tp"),
            P("tp", None),
            P("tp"),
            P("tp"),
        ),
        out_specs=P("dp", ("sp", "tp"), None),
        check_vma=False,
    )
```

profile of v0, /device:TPU:28, one launch (start us, length us, event | category | flops | bytes accessed | tf_op | source)
XLA Modules:
  0.0 63.4 jit_solution(549966415182104980)
XLA Ops:
  0.0 60.2 %shard_map.136 = bf16[2,256,2048]{2,1,0:T(8,128)(2,1)} custom-call(bf16[2,1024,2048]{2,1,0:T(8,128)(2,1)} %latent.1, bf16[2,256,2048]{2,1,0:T(8,128)(2,1)} %context.1, bf16[2,512]{1,0:T(2,128)(2,1)} %condition.1, bf16[512]{0:T(512)(128)(2,1)} %ctx_cond.1, f32[1,2048]{1,0:T(1,128)} %bitcast.5, bf16[512,512]{1,0:T(8,128)(2,1)} %w_shift.1, ...), custom_call_target="tpu_custom_call" | custom-call | tf_op jit(solution)/shard_map/pallas_call | solution.py:491
  60.2 3.2 %copy.16 = bf16[2,256,2048]{2,1,0:T(8,128)(2,1)} copy(bf16[2,256,2048]{2,1,0:T(8,128)(2,1)} %shard_map.136) | data formatting | bytes 4194304
where the time goes:
time: 63.5 us; the launch traced here: 63.4 us
  Pallas kernels  60.2 us (95%)
  local copies, waits for them, and re-layouts  3.16 us (5%)
    pallas_call x1, Pallas kernels, shards(): pl.pallas_call(functools.partial(kernel, (n_sp, n_tp, n_dp)), out_shape=j...  60.2 us
    unnamed x1, local copies, waits for them, and re-layouts  3.16 us

commit v1 on v0

v1 whole, which is shorter than its diff:
```python
import functools
import math

import jax
import jax.numpy as jnp
from jax import lax
from jax.experimental import pallas as pl
from jax.experimental.pallas import tpu as pltpu
from jax.sharding import PartitionSpec as P

HEAD = 64
WINDOW = 128
GRID_COLS = 64
LANES = 128
ONES = 16

epsilon = 1e-06
rope_base = 10000.0
masked_value = -1e30
log2e = 1.4426950408889634
MESH = pl.DeviceIdType.MESH
nt = (((1,), (1,)), ((), ()))
f32 = jnp.float32
bf16 = jnp.bfloat16


def kernel(
    sizes,
    latent,
    context,
    condition,
    ctx_cond,
    norm_gain,
    w_shift,
    w_scale,
    w_gate,
    w_query,
    w_key,
    w_value,
    w_out,
    sink_logit,
    ctx_lift,
    out,
    x_lat,
    x_ctx,
    w_mod,
    w_q,
    w_t,
    w_s,
    w_c,
    cos_row,
    sin_row,
    cos_col,
    sin_col,
    w_o,
    act,
    mod_rx,
    mod_all,
    gate_rx,
    gate_all,
    vec_a,
    vec_b,
    vec_g,
    inv_lat,
    inv_ctx,
    bias_col,
    bias_row,
    q_buf,
    kv_buf,
    vt_buf,
    ckv_buf,
    cvt_buf,
    mask_buf,
    s_a,
    s_b,
    att_buf,
    rows_rx,
    ld_sem,
    ma_send,
    ma_recv,
    mb_send,
    mb_recv,
    ga_send,
    ga_recv,
    gb_send,
    gb_recv,
    cx_send,
    cx_recv,
    ha_send,
    ha_recv,
    at_send,
    at_recv,
    wo_send,
    wo_recv,
    wf_send,
    wf_recv,
):
    n_sp, n_tp, n_dp = sizes
    me_sp, me_tp, me_dp = lax.axis_index("sp"), lax.axis_index("tp"), lax.axis_index("dp")
    samples, tokens, width = latent.shape
    ctx_rows = context.shape[1]
    ctx_all = n_sp * ctx_rows
    part = w_shift.shape[1]
    q_cols = w_query.shape[1]
    heads = q_cols // HEAD
    block = tokens // n_tp
    quarter = HEAD // 4
    q_scale = log2e * HEAD ** (-0.5)

    def other(me, step, count):
        return lax.rem(me + step, count)

    barrier = pltpu.get_barrier_semaphore()
    for axis, me, count in (("sp", me_sp, n_sp), ("tp", me_tp, n_tp), ("dp", me_dp, n_dp)):
        for step in range(1, count):
            pl.semaphore_signal(
                barrier, inc=1, device_id={axis: other(me, step, count)}, device_id_type=MESH
            )

    loads = []
    for source, target in (
        (w_shift, w_mod.at[0]),
        (w_scale, w_mod.at[1]),
        (context, x_ctx),
        (w_key, w_t.at[q_cols : q_cols + HEAD]),
        (w_value, w_t.at[q_cols + HEAD : q_cols + 2 * HEAD]),
        (w_query, w_q),
        (w_gate, w_mod.at[2]),
        *((latent.at[s], x_lat.at[s]) for s in range(samples)),
        (w_out, w_o.at[me_tp]),
    ):
        copy = pltpu.make_async_copy(source, target, ld_sem.at[len(loads)])
        copy.start()
        loads.append(copy)

    def peers(axis, me, count, buffer, send, recv):
        def copy(step, source):
            return pltpu.make_async_remote_copy(
                src_ref=buffer.at[source],
                dst_ref=buffer.at[source],
                send_sem=send.at[step],
                recv_sem=recv.at[step],
                device_id={axis: other(me, step, count)},
                device_id_type=MESH,
            )

        def start():
            for step in range(1, count):
                copy(step, me).start()

        def arrive():
            for step in range(1, count):
                copy(step, other(me, count - step, count)).wait_recv()

        def finish():
            for step in range(1, count):
                copy(step, me).wait_send()

        return start, arrive, finish

    mod_a = peers("sp", me_sp, n_sp, mod_rx, ma_send, ma_recv)
    mod_b = peers("tp", me_tp, n_tp, mod_all, mb_send, mb_recv)
    gate_a = peers("sp", me_sp, n_sp, gate_rx, ga_send, ga_recv)
    gate_b = peers("tp", me_tp, n_tp, gate_all, gb_send, gb_recv)
    keep_rows = mod_rx.shape[1]

    act[...] = jnp.zeros_like(act)
    cond = condition[...].astype(f32)
    act[0:samples, :] = cond / (1.0 + jnp.exp(-cond))
    cond = ctx_cond[...].astype(f32).reshape(1, -1)
    act[samples : samples + 1, :] = cond / (1.0 + jnp.exp(-cond))
    active = act[...].astype(bf16)
    for i in range(2):
        loads[i].wait()
        mod_rx[me_sp, :, i * part : (i + 1) * part] = jnp.dot(
            active, w_mod[i], preferred_element_type=f32
        )[0:keep_rows]
    pl.semaphore_wait(barrier, n_sp + n_tp + n_dp - 3)
    mod_a[0]()

    loads[6].wait()
    gate_rx[me_sp] = jnp.dot(active, w_mod[2], preferred_element_type=f32)[0:keep_rows]
    gate_a[0]()

    loads[2].wait()
    for s in range(samples):
        wide = x_ctx[s].astype(f32)
        total = jnp.sum(wide * wide, axis=-1, keepdims=True)
        inv_ctx[s] = jnp.broadcast_to(lax.rsqrt(total / width + epsilon), (ctx_rows, LANES))

    loads[3].wait()
    loads[4].wait()
    loads[5].wait()
    for i in range(0, width, 256):
        w_t[0:q_cols, i : i + 256] = w_q[i : i + 256, :].T

    fill_tables(me_sp * (tokens // GRID_COLS), cos_row, sin_row, cos_col, sin_col)
    key_id = lax.broadcasted_iota(jnp.int32, (WINDOW, LANES), 0)
    query_id = lax.broadcasted_iota(jnp.int32, (WINDOW, LANES), 1)
    mask_buf[0] = jnp.where(key_id >= query_id, 0.0, masked_value)
    mask_buf[1] = jnp.where(key_id <= query_id, 0.0, masked_value)
    q_buf[:, :, HEAD:, :] = jnp.zeros(q_buf.shape[:2] + (LANES - HEAD, tokens), bf16)
    vt_buf[:, HEAD:, :] = jnp.ones((samples, ONES, vt_buf.shape[2]), bf16)
    cvt_buf[:, HEAD:, :] = jnp.ones((samples, ONES, ctx_all), bf16)
    vec_b[...] = jnp.zeros_like(vec_b)

    def stats(s):
        def body(i, carry):
            rows = pl.ds(pl.multiple_of(i * block, block), block)
            wide = x_lat[s, rows, :].astype(f32)
            acc = wide[:, 0:LANES] * wide[:, 0:LANES]
            for k in range(LANES, width, LANES):
                acc = acc + wide[:, k : k + LANES] * wide[:, k : k + LANES]
            total = jnp.sum(acc.T, axis=0, keepdims=True)
            inv_lat[s, :, rows] = lax.rsqrt(total / width + epsilon)
            return carry

        lax.fori_loop(0, n_tp, body, 0)

    loads[7].wait()
    stats(0)

    mod_a[1]()
    total = mod_rx[0]
    for i in range(1, n_sp):
        total = total + mod_rx[i]
    mod_all[me_tp] = total
    mod_b[0]()

    for s in range(1, samples):
        loads[7 + s].wait()
        stats(s)

    gate_a[1]()
    total = gate_rx[0]
    for i in range(1, n_sp):
        total = total + gate_rx[i]
    gate_all[me_tp] = total
    gate_b[0]()

    mod_b[1]()
    for t in range(n_tp):
        cols = slice(t * part, (t + 1) * part)
        vec_b[0:keep_rows, cols] = mod_all[t, :, 0:part]
        vec_a[0:keep_rows, cols] = (1.0 + mod_all[t, :, part : 2 * part]) * norm_gain[:, cols]

    share = w_out.shape[0] // n_dp
    mine = pl.ds(pl.multiple_of(me_dp * share, share), share)

    def out_copy(step, source):
        return pltpu.make_async_remote_copy(
            src_ref=w_out.at[mine, :],
            dst_ref=w_o.at[source, mine, :],
            send_sem=wo_send.at[step],
            recv_sem=wo_recv.at[step],
            device_id={"tp": other(me_tp, step, n_tp)},
            device_id_type=MESH,
        )

    def forward_copy(step, hop, part_id):
        source = other(me_tp, n_tp - step, n_tp)
        rows = pl.ds(pl.multiple_of(part_id * share, share), share)
        return pltpu.make_async_remote_copy(
            src_ref=w_o.at[source, rows, :],
            dst_ref=w_o.at[source, rows, :],
            send_sem=wf_send.at[step, hop],
            recv_sem=wf_recv.at[step, hop],
            device_id={"dp": other(me_dp, hop, n_dp)},
            device_id_type=MESH,
        )

    for step in range(1, n_tp):
        out_copy(step, me_tp).start()

    def fold(target, first, last, base, row):
        gain = vec_a[row : row + 1, :]
        for r in range(first, last, 32):
            target[r - base : r - base + 32, :] = (w_t[r : r + 32, :].astype(f32) * gain).astype(bf16)

    shift = vec_b[...]
    high = shift.astype(bf16).astype(f32)
    shift_pair = jnp.concatenate([high, shift - high], axis=0).astype(bf16)
    bias = lax.dot_general(shift_pair, w_t[q_cols:, :], nt, preferred_element_type=f32)
    bias_row[...] = bias[0:8] + bias[8:16]
    fold(w_c, q_cols, q_cols + 2 * HEAD, q_cols, samples)

    def ctx_copy(s, step, source):
        rows = pl.ds(pl.multiple_of(source * ctx_rows, ctx_rows), ctx_rows)
        return pltpu.make_async_remote_copy(
            src_ref=ckv_buf.at[s, rows, :],
            dst_ref=ckv_buf.at[s, rows, :],
            send_sem=cx_send.at[s, step],
            recv_sem=cx_recv.at[s, step],
            device_id={"sp": other(me_sp, step, n_sp)},
            device_id_type=MESH,
        )

    for s in range(samples):
        rows = pl.ds(pl.multiple_of(me_sp * ctx_rows, ctx_rows), ctx_rows)
        kv = lax.dot_general(x_ctx[s], w_c[...], nt, preferred_element_type=f32)
        ckv_buf[s, rows, :] = (kv * inv_ctx[s] + bias_row[samples : samples + 1, :]).astype(bf16)
        for step in range(1, n_sp):
            ctx_copy(s, step, me_sp).start()

    bias = lax.dot_general(w_t[...], shift_pair, nt, preferred_element_type=f32)
    for s in range(samples):
        column = bias[:, s : s + 1] + bias[:, 8 + s : 9 + s]
        bias_col[s, 0:q_cols, :] = jnp.broadcast_to(column[0:q_cols] * q_scale, (q_cols, LANES))
        bias_col[s, q_cols:, :] = jnp.broadcast_to(column[q_cols:], (2 * HEAD, LANES))
        fold(w_s.at[s], 0, q_cols + 2 * HEAD, 0, s)

    def halo_copy(s, side):
        source, target = ((tokens, 0), (WINDOW, WINDOW + tokens))[side]
        step = (1, n_sp - 1)[side]
        return pltpu.make_async_remote_copy(
            src_ref=kv_buf.at[s, pl.ds(source, WINDOW), :],
            dst_ref=kv_buf.at[s, pl.ds(target, WINDOW), :],
            send_sem=ha_send.at[s, side],
            recv_sem=ha_recv.at[s, side],
            device_id={"sp": other(me_sp, step, n_sp)},
            device_id_type=MESH,
        )

    def project(s, start):
        cols = slice(start, start + block)
        y = lax.dot_general(w_s[s], x_lat[s, cols, :], nt, preferred_element_type=f32)
        inv = inv_lat[s, :, cols]
        inv_q = inv * q_scale
        cr, sr = cos_row[:, cols], sin_row[:, cols]
        cc, sc = cos_col[...], sin_col[...]

        def wide(first, count):
            return jnp.concatenate([bias_col[s, first : first + count, :]] * (block // LANES), axis=1)

        def rotated(base, scale):
            u = [
                y[base + k * quarter : base + (k + 1) * quarter] * scale
                + wide(base + k * quarter, quarter)
                for k in range(4)
            ]
            return (
                u[0] * cr - u[1] * sr,
                u[0] * sr + u[1] * cr,
                u[2] * cc - u[3] * sc,
                u[2] * sc + u[3] * cc,
            )

        for h in range(heads):
            q_buf[s, h, 0:HEAD, cols] = jnp.concatenate(rotated(h * HEAD, inv_q), axis=0).astype(bf16)
        v = y[q_cols + HEAD :] * inv + wide(q_cols + HEAD, HEAD)
        kv = jnp.concatenate((*rotated(q_cols, inv), v), axis=0)
        vt_buf[s, 0:HEAD, WINDOW + start : WINDOW + start + block] = v.astype(bf16)
        kv_buf[s, WINDOW + start : WINDOW + start + block, :] = kv.T.astype(bf16)

    for s in range(samples):
        for i in range(n_tp):
            project(s, i * block)
        halo_copy(s, 0).start()
        halo_copy(s, 1).start()

    def rows_copy(s, step, source):
        target = other(me_tp, step, n_tp)
        return pltpu.make_async_remote_copy(
            src_ref=att_buf.at[s, target],
            dst_ref=rows_rx.at[source, s],
            send_sem=at_send.at[s, step],
            recv_sem=at_recv.at[s, step],
            device_id={"tp": target},
            device_id_type=MESH,
        )

    pairs = heads // 2
    halves = block // LANES
    near_rows = LANES + 2 * WINDOW
    low = lax.broadcasted_iota(jnp.int32, (1, 2 * LANES), 1) < LANES

    def two(ref, pair):
        return jnp.where(low, ref[2 * pair], ref[2 * pair + 1]) * log2e

    def start_of(index):
        step = index // halves + 1
        owner = other(me_tp, step, n_tp)
        return pl.multiple_of(owner * block + (index % halves) * LANES, LANES)

    chunks = [(False, 0, 2 * WINDOW), (False, 2 * WINDOW, LANES)]
    far_chunk = min(256, ctx_all)
    for c in range(0, ctx_all, far_chunk):
        chunks.append((True, c, far_chunk))

    def score_steps(s, index, pair, buf, state):
        start = start_of(index)
        cols = pl.ds(start, LANES)
        q = jnp.concatenate(
            [q_buf[s, 2 * pair, :, cols], q_buf[s, 2 * pair + 1, :, cols]], axis=1
        )
        tops = [None, None]

        def one(chunk):
            far, first, count = chunk
            if far:
                keys = ckv_buf[s, first : first + count, :]
            else:
                keys = kv_buf[s, pl.ds(start + first, count), :]
            scores = jnp.dot(keys, q, preferred_element_type=f32)
            base = near_rows + first if far else first
            if not far:
                mask = mask_buf[0 if first == 0 else 1]
                mask = jnp.concatenate([mask, mask], axis=1)
                edge = scores[0:WINDOW] + mask
                if count > WINDOW:
                    scores = jnp.concatenate([edge, scores[WINDOW:]], axis=0)
                else:
                    scores = edge
            buf[base : base + count, :] = scores
            high = jnp.max(scores.reshape(count // 8, 8, 2 * LANES), axis=0)
            tops[far] = high if tops[far] is None else jnp.maximum(tops[far], high)

        for chunk in chunks:
            yield functools.partial(one, chunk)

        def close():
            near_top = jnp.max(tops[0], axis=0, keepdims=True)
            far_top = jnp.max(tops[1], axis=0, keepdims=True)
            lift = two(ctx_lift, pair)
            state.append(
                jnp.maximum(jnp.maximum(near_top, far_top + lift), two(sink_logit, pair))
            )

        yield close

    def value_steps(s, index, pair, buf, top):
        start = start_of(index)
        far_top = top - two(ctx_lift, pair)
        acc = [None]

        def one(chunk):
            far, first, count = chunk
            base = near_rows + first if far else first
            p = jnp.exp2(buf[base : base + count, :] - (far_top if far else top)).astype(bf16)
            if far:
                values = cvt_buf[s, :, first : first + count]
            else:
                values = vt_buf[s, :, pl.ds(start + first, count)]
            term = jnp.dot(values, p, preferred_element_type=f32)
            acc[0] = term if acc[0] is None else acc[0] + term

        for chunk in chunks:
            yield functools.partial(one, chunk)

        def close():
            weight = acc[0][HEAD : HEAD + 1] + jnp.exp2(two(sink_logit, pair) - top)
            rows = acc[0][0:HEAD] * (1.0 / weight)
            stacked = jnp.concatenate([rows[:, 0:LANES], rows[:, LANES:]], axis=0)
            owner = other(me_tp, index // halves + 1, n_tp)
            half = pl.multiple_of((index % halves) * LANES, LANES)
            att_buf[s, owner, pl.ds(half, LANES), pair * LANES : (pair + 1) * LANES] = (
                stacked.T.astype(bf16)
            )

        yield close

    def run(*streams):
        for steps in zip(*streams):
            for step in steps:
                step()

    bufs = (s_a, s_b)

    def attention(s):
        count = n_tp * halves
        top0 = []
        run(score_steps(s, 0, 0, s_a, top0))

        def body(index, top, last):
            for pair in range(pairs):
                mine_buf, next_buf = bufs[pair % 2], bufs[(pair + 1) % 2]
                fresh = []
                streams = [value_steps(s, index, pair, mine_buf, top)]
                if pair + 1 < pairs:
                    streams.insert(0, score_steps(s, index, pair + 1, next_buf, fresh))
                elif not last:
                    streams.insert(0, score_steps(s, index + 1, 0, next_buf, fresh))
                run(*streams)
                top = fresh[0] if fresh else top

            step = index // halves + 1

            @pl.when((index % halves == halves - 1) & (step < n_tp))
            def _():
                rows_copy(s, step, me_tp).start()

            return top

        top = lax.fori_loop(0, count - 1, lambda i, top: body(i, top, False), top0[0])
        body(count - 1, top, True)
        rows_rx[me_tp, s] = att_buf[s, me_tp]

    def context_ready(s):
        for step in range(1, n_sp):
            ctx_copy(s, step, other(me_sp, n_sp - step, n_sp)).wait_recv()
        for c in range(0, ctx_all, 256):
            cvt_buf[s, 0:HEAD, c : c + 256] = ckv_buf[s, c : c + 256, :].T[HEAD:]

    def halo_ready(s):
        for side in range(2):
            halo_copy(s, side).wait_recv()
            first = (0, WINDOW + tokens)[side]
            valid = (me_sp > 0, me_sp < n_sp - 1)[side]
            rows = jnp.where(valid, kv_buf[s, first : first + WINDOW, :].astype(f32), 0.0)
            kv_buf[s, first : first + WINDOW, :] = rows.astype(bf16)
            vt_buf[s, 0:HEAD, first : first + WINDOW] = rows.T[HEAD:].astype(bf16)
            vt_buf[s, HEAD:, first : first + WINDOW] = jnp.where(
                valid, jnp.ones((ONES, WINDOW), f32), 0.0
            ).astype(bf16)

    for s in range(samples):
        halo_ready(s)
        context_ready(s)
        attention(s)
        if s == 0:
            for step in range(1, n_tp):
                out_copy(step, other(me_tp, n_tp - step, n_tp)).wait_recv()
                for hop in range(1, n_dp):
                    forward_copy(step, hop, me_dp).start()

    gate_b[1]()
    for t in range(n_tp):
        vec_g[0:keep_rows, t * part : (t + 1) * part] = gate_all[t]

    loads[-1].wait()
    for step in range(1, n_tp):
        for hop in range(1, n_dp):
            forward_copy(step, hop, other(me_dp, n_dp - hop, n_dp)).wait_recv()
    chunk = 512
    for s in range(samples):
        for step in range(1, n_tp):
            rows_copy(s, step, other(me_tp, n_tp - step, n_tp)).wait_recv()

        def finish(i, carry):
            cols = pl.ds(pl.multiple_of(i * chunk, chunk), chunk)
            acc = jnp.dot(rows_rx[0, s], w_o[0, :, cols], preferred_element_type=f32)
            for t in range(1, n_tp):
                acc += jnp.dot(rows_rx[t, s], w_o[t, :, cols], preferred_element_type=f32)
            out[s, :, cols] = (acc * vec_g[s : s + 1, cols]).astype(bf16)
            return carry

        lax.fori_loop(0, width // chunk, finish, 0)

    for _, _, finish_send in (mod_a, mod_b, gate_a, gate_b):
        finish_send()
    for s in range(samples):
        for step in range(1, n_sp):
            ctx_copy(s, step, me_sp).wait_send()
        halo_copy(s, 0).wait_send()
        halo_copy(s, 1).wait_send()
    for step in range(1, n_tp):
        out_copy(step, me_tp).wait_send()
        for hop in range(1, n_dp):
            forward_copy(step, hop, me_dp).wait_send()
        for s in range(samples):
            rows_copy(s, step, me_tp).wait_send()


def fill_tables(first_row, cos_row, sin_row, cos_col, sin_col):
    tokens = cos_row.shape[1]
    quarter = HEAD // 4

    def pair(ticks, shape):
        power = lax.broadcasted_iota(jnp.int32, shape, 0).astype(f32)
        angles = ticks.astype(f32) * jnp.exp(power * (-math.log(rope_base) / quarter))
        return jnp.cos(angles), jnp.sin(angles)

    shape = cos_col.shape
    token = lax.broadcasted_iota(jnp.int32, shape, 1)
    cos_col[...], sin_col[...] = pair(token % GRID_COLS, shape)
    lines = tokens // GRID_COLS
    shape = (quarter, LANES)
    for first in range(0, lines, LANES):
        line = lax.broadcasted_iota(jnp.int32, shape, 1) + first + first_row
        cos_all, sin_all = pair(line, shape)
        half = lax.broadcasted_iota(jnp.int32, shape, 1) < GRID_COLS
        for r in range(0, min(LANES, lines - first), 2):
            cols = slice((first + r) * GRID_COLS, (first + r + 2) * GRID_COLS)
            for source, target in ((cos_all, cos_row), (sin_all, sin_row)):
                target[:, cols] = jnp.where(half, source[:, r : r + 1], source[:, r + 1 : r + 2])


def shards(
    latent,
    context,
    condition,
    ctx_cond,
    norm_gain,
    w_shift,
    w_scale,
    w_gate,
    w_query,
    w_key,
    w_value,
    w_out,
    sink_logit,
    ctx_lift,
):
    samples, tokens, width = latent.shape
    ctx_rows = context.shape[1]
    n_sp, n_tp, n_dp = lax.axis_size("sp"), lax.axis_size("tp"), lax.axis_size("dp")
    q_cols = w_query.shape[1]
    heads = q_cols // HEAD
    assert w_key.shape[1] == HEAD and tokens % GRID_COLS == 0 and samples < 4 and heads % 4 == 0
    part = w_shift.shape[1]
    block = tokens // n_tp
    ctx_all = n_sp * ctx_rows
    vmem = pl.BlockSpec(memory_space=pltpu.VMEM)
    smem = pl.BlockSpec(memory_space=pltpu.SMEM)
    anywhere = pl.BlockSpec(memory_space=pl.ANY)
    dma = pltpu.SemaphoreType.DMA
    padded = tokens + 2 * WINDOW
    proj = q_cols + 2 * HEAD
    keys = LANES + 2 * WINDOW + ctx_all
    V = pltpu.VMEM
    return pl.pallas_call(
        functools.partial(kernel, (n_sp, n_tp, n_dp)),
        out_shape=jax.ShapeDtypeStruct((samples, block, width), bf16),
        in_specs=[anywhere] * 2 + [vmem] * 3 + [anywhere] * 7 + [smem] * 2,
        out_specs=vmem,
        scratch_shapes=[
            V(latent.shape, bf16),
            V(context.shape, bf16),
            V((3,) + w_shift.shape, bf16),
            V(w_query.shape, bf16),
            V((proj, width), bf16),
            V((samples, proj, width), bf16),
            V((2 * HEAD, width), bf16),
            V((HEAD // 4, tokens), f32),
            V((HEAD // 4, tokens), f32),
            V((HEAD // 4, block), f32),
            V((HEAD // 4, block), f32),
            V((n_tp,) + w_out.shape, bf16),
            V((8, w_shift.shape[0]), f32),
            V((n_sp, 4, 2 * part), f32),
            V((n_tp, 4, 2 * part), f32),
            V((n_sp, 4, part), f32),
            V((n_tp, 4, part), f32),
            V((8, width), f32),
            V((8, width), f32),
            V((8, width), f32),
            V((samples, 1, tokens), f32),
            V((samples, ctx_rows, LANES), f32),
            V((samples, proj, LANES), f32),
            V((8, 2 * HEAD), f32),
            V((samples, heads, LANES, tokens), bf16),
            V((samples, padded, LANES), bf16),
            V((samples, HEAD + ONES, padded), bf16),
            V((samples, ctx_all, LANES), bf16),
            V((samples, HEAD + ONES, ctx_all), bf16),
            V((2, WINDOW, LANES), f32),
            V((keys, 2 * LANES), f32),
            V((keys, 2 * LANES), f32),
            V((samples, n_tp, block, q_cols), bf16),
            V((n_tp, samples, block, q_cols), bf16),
            dma((8 + samples,)),
            dma((n_sp,)),
            dma((n_sp,)),
            dma((n_tp,)),
            dma((n_tp,)),
            dma((n_sp,)),
            dma((n_sp,)),
            dma((n_tp,)),
            dma((n_tp,)),
            dma((samples, n_sp)),
            dma((samples, n_sp)),
            dma((samples, 2)),
            dma((samples, 2)),
            dma((samples, n_tp)),
            dma((samples, n_tp)),
            dma((n_tp,)),
            dma((n_tp,)),
            dma((n_tp, n_dp)),
            dma((n_tp, n_dp)),
        ],
        compiler_params=pltpu.CompilerParams(
            collective_id=0, has_side_effects=True, vmem_limit_bytes=60 * 1024 * 1024
        ),
    )(
        latent,
        context,
        condition,
        ctx_cond,
        norm_gain.reshape(1, -1),
        w_shift,
        w_scale,
        w_gate,
        w_query,
        w_key.T,
        w_value.T,
        w_out,
        sink_logit,
        ctx_lift,
    )


def solution(mesh):
    return jax.shard_map(
        shards,
        mesh=mesh,
        in_specs=(
            P("dp", "sp", None),
            P("dp", "sp", None),
            P("dp", "sp"),
            P("sp"),
            P(),
            P("sp", "tp"),
            P("sp", "tp"),
            P("sp", "tp"),
            P(None, "tp"),
            P(None, "tp"),
            P(None, "tp"),
            P("tp", None),
            P("tp"),
            P("tp"),
        ),
        out_specs=P("dp", ("sp", "tp"), None),
        check_vma=False,
    )
```

time: 63.5 us -> 56.8 us (0.89)
  the two profiles are of different devices: /device:TPU:28 before, /device:TPU:0 now
where the time goes in v1:
time: 56.8 us; the launch traced here: 56.6 us
  Pallas kernels  53.5 us (94%)
  local copies, waits for them, and re-layouts  3.16 us (6%)
    pallas_call x1, Pallas kernels, shards(): pl.pallas_call(functools.partial(kernel, (n_sp, n_tp, n_dp)), out_shape=j...  53.5 us
    unnamed x1, local copies, waits for them, and re-layouts  3.16 us

profile of v1, /device:TPU:0, one launch (start us, length us, event | category | flops | bytes accessed | tf_op | source)
XLA Modules:
  0.0 56.6 jit_solution(271387345432746711)
XLA Ops:
  0.0 53.5 %shard_map.136 = bf16[2,256,2048]{2,1,0:T(8,128)(2,1)} custom-call(bf16[2,1024,2048]{2,1,0:T(8,128)(2,1)} %latent.1, bf16[2,256,2048]{2,1,0:T(8,128)(2,1)} %context.1, bf16[2,512]{1,0:T(2,128)(2,1)} %condition.1, bf16[512]{0:T(512)(128)(2,1)} %ctx_cond.1, f32[1,2048]{1,0:T(1,128)} %bitcast.5, bf16[512,512]{1,0:T(8,128)(2,1)} %w_shift.1, ...), custom_call_target="tpu_custom_call" | custom-call | tf_op jit(solution)/shard_map/pallas_call | solution.py:621
  53.5 3.2 %copy.16 = bf16[2,256,2048]{2,1,0:T(8,128)(2,1)} copy(bf16[2,256,2048]{2,1,0:T(8,128)(2,1)} %shard_map.136) | data formatting | bytes 4194304

commit v2 on v1

--- a/solution.py
+++ b/solution.py
@@ -13,6 +13,7 @@
 GRID_COLS = 64
 LANES = 128
 ONES = 16
+PIECES = 4
 
 epsilon = 1e-06
 rope_base = 10000.0
@@ -164,6 +165,51 @@
     gate_b = peers("tp", me_tp, n_tp, gate_all, gb_send, gb_recv)
     keep_rows = mod_rx.shape[1]
 
+    share = w_out.shape[0] // n_dp
+    piece = share // PIECES
+    across = me_tp + 1 - 2 * lax.rem(me_tp, 2)
+    along = lax.rem(me_tp + 2, n_tp)
+    diagonal = lax.rem(across + 2, n_tp)
+
+    def piece_copy(kind, i, source, target, local):
+        rows = pl.ds(pl.multiple_of(me_dp * share + i * piece, piece), piece)
+        return pltpu.make_async_remote_copy(
+            src_ref=local.at[rows, :],
+            dst_ref=w_o.at[source, rows, :],
+            send_sem=wo_send.at[kind, i],
+            recv_sem=wo_recv.at[kind, i],
+            device_id={"tp": target},
+            device_id_type=MESH,
+        )
+
+    def own_copy(kind, i):
+        return piece_copy(kind, i, me_tp, (across, along)[kind], w_out)
+
+    def relay_copy(i):
+        source, target = ((across, along), (along, across))[2 * i // PIECES]
+        return piece_copy(2, i, source, target, w_o.at[source])
+
+    def piece_arrive(kind, i):
+        source = (across, along, diagonal)[kind]
+        target = (across, along, (along, across)[2 * i // PIECES])[kind]
+        piece_copy(kind, i, source, target, w_o.at[source]).wait_recv()
+
+    def relay(first, last):
+        for i in range(first, last):
+            piece_arrive(2 * i // PIECES, i)
+            relay_copy(i).start()
+
+    def forward_copy(source, index, hop, part_id):
+        rows = pl.ds(pl.multiple_of(part_id * share, share), share)
+        return pltpu.make_async_remote_copy(
+            src_ref=w_o.at[source, rows, :],
+            dst_ref=w_o.at[source, rows, :],
+            send_sem=wf_send.at[index, hop],
+            recv_sem=wf_recv.at[index, hop],
+            device_id={"dp": other(me_dp, hop, n_dp)},
+            device_id_type=MESH,
+        )
+
     act[...] = jnp.zeros_like(act)
     cond = condition[...].astype(f32)
     act[0:samples, :] = cond / (1.0 + jnp.exp(-cond))
@@ -177,6 +223,8 @@
         )[0:keep_rows]
     pl.semaphore_wait(barrier, n_sp + n_tp + n_dp - 3)
     mod_a[0]()
+    own_copy(0, 0).start()
+    own_copy(1, 0).start()
 
     loads[6].wait()
     gate_rx[me_sp] = jnp.dot(active, w_mod[2], preferred_element_type=f32)[0:keep_rows]
@@ -226,6 +274,9 @@
         total = total + mod_rx[i]
     mod_all[me_tp] = total
     mod_b[0]()
+    for i in range(1, PIECES):
+        own_copy(0, i).start()
+        own_copy(1, i).start()
 
     for s in range(1, samples):
         loads[7 + s].wait()
@@ -243,34 +294,6 @@
         cols = slice(t * part, (t + 1) * part)
         vec_b[0:keep_rows, cols] = mod_all[t, :, 0:part]
         vec_a[0:keep_rows, cols] = (1.0 + mod_all[t, :, part : 2 * part]) * norm_gain[:, cols]
-
-    share = w_out.shape[0] // n_dp
-    mine = pl.ds(pl.multiple_of(me_dp * share, share), share)
-
-    def out_copy(step, source):
-        return pltpu.make_async_remote_copy(
-            src_ref=w_out.at[mine, :],
-            dst_ref=w_o.at[source, mine, :],
-            send_sem=wo_send.at[step],
-            recv_sem=wo_recv.at[step],
-            device_id={"tp": other(me_tp, step, n_tp)},
-            device_id_type=MESH,
-        )
-
-    def forward_copy(step, hop, part_id):
-        source = other(me_tp, n_tp - step, n_tp)
-        rows = pl.ds(pl.multiple_of(part_id * share, share), share)
-        return pltpu.make_async_remote_copy(
-            src_ref=w_o.at[source, rows, :],
-            dst_ref=w_o.at[source, rows, :],
-            send_sem=wf_send.at[step, hop],
-            recv_sem=wf_recv.at[step, hop],
-            device_id={"dp": other(me_dp, hop, n_dp)},
-            device_id_type=MESH,
-        )
-
-    for step in range(1, n_tp):
-        out_copy(step, me_tp).start()
 
     def fold(target, first, last, base, row):
         gain = vec_a[row : row + 1, :]
@@ -295,19 +318,24 @@
             device_id_type=MESH,
         )
 
-    for s in range(samples):
+    def context_keys(s):
         rows = pl.ds(pl.multiple_of(me_sp * ctx_rows, ctx_rows), ctx_rows)
         kv = lax.dot_general(x_ctx[s], w_c[...], nt, preferred_element_type=f32)
         ckv_buf[s, rows, :] = (kv * inv_ctx[s] + bias_row[samples : samples + 1, :]).astype(bf16)
         for step in range(1, n_sp):
             ctx_copy(s, step, me_sp).start()
 
-    bias = lax.dot_general(w_t[...], shift_pair, nt, preferred_element_type=f32)
-    for s in range(samples):
-        column = bias[:, s : s + 1] + bias[:, 8 + s : 9 + s]
-        bias_col[s, 0:q_cols, :] = jnp.broadcast_to(column[0:q_cols] * q_scale, (q_cols, LANES))
-        bias_col[s, q_cols:, :] = jnp.broadcast_to(column[q_cols:], (2 * HEAD, LANES))
+    context_keys(0)
+
+    def fold_sample(s):
         fold(w_s.at[s], 0, q_cols + 2 * HEAD, 0, s)
+        bias_col[s, 0:q_cols, :] = jnp.broadcast_to(column[0:q_cols, s : s + 1] * q_scale, (q_cols, LANES))
+        bias_col[s, q_cols:, :] = jnp.broadcast_to(column[q_cols:, s : s + 1], (2 * HEAD, LANES))
+
+    bias = lax.dot_general(shift_pair, w_t[0:q_cols, :], nt, preferred_element_type=f32)
+    bias = jnp.concatenate([bias[0:8] + bias[8:16], bias_row[...]], axis=1)
+    bias = jnp.concatenate([bias, jnp.zeros((LANES - 8, bias.shape[1]), f32)], axis=0)
+    column = bias.T
 
     def halo_copy(s, side):
         source, target = ((tokens, 0), (WINDOW, WINDOW + tokens))[side]
@@ -353,10 +381,15 @@
         kv_buf[s, WINDOW + start : WINDOW + start + block, :] = kv.T.astype(bf16)
 
     for s in range(samples):
+        if s > 0:
+            context_keys(s)
+        fold_sample(s)
         for i in range(n_tp):
             project(s, i * block)
         halo_copy(s, 0).start()
         halo_copy(s, 1).start()
+        if s < 2:
+            relay(s * PIECES // 2, (s + 1) * PIECES // 2)
 
     def rows_copy(s, step, source):
         target = other(me_tp, step, n_tp)
@@ -518,19 +551,21 @@
         context_ready(s)
         attention(s)
         if s == 0:
-            for step in range(1, n_tp):
-                out_copy(step, other(me_tp, n_tp - step, n_tp)).wait_recv()
+            for index, source in enumerate((across, along, diagonal)):
+                for i in range(PIECES):
+                    if index == 2 or 2 * i // PIECES != index:
+                        piece_arrive(index, i)
                 for hop in range(1, n_dp):
-                    forward_copy(step, hop, me_dp).start()
+                    forward_copy(source, index, hop, me_dp).start()
 
     gate_b[1]()
     for t in range(n_tp):
         vec_g[0:keep_rows, t * part : (t + 1) * part] = gate_all[t]
 
     loads[-1].wait()
-    for step in range(1, n_tp):
+    for index, source in enumerate((across, along, diagonal)):
         for hop in range(1, n_dp):
-            forward_copy(step, hop, other(me_dp, n_dp - hop, n_dp)).wait_recv()
+            forward_copy(source, index, hop, other(me_dp, n_dp - hop, n_dp)).wait_recv()
     chunk = 512
     for s in range(samples):
         for step in range(1, n_tp):
@@ -553,10 +588,14 @@
             ctx_copy(s, step, me_sp).wait_send()
         halo_copy(s, 0).wait_send()
         halo_copy(s, 1).wait_send()
+    for i in range(PIECES):
+        own_copy(0, i).wait_send()
+        own_copy(1, i).wait_send()
+        relay_copy(i).wait_send()
+    for index, source in enumerate((across, along, diagonal)):
+        for hop in range(1, n_dp):
+            forward_copy(source, index, hop, me_dp).wait_send()
     for step in range(1, n_tp):
-        out_copy(step, me_tp).wait_send()
-        for hop in range(1, n_dp):
-            forward_copy(step, hop, me_dp).wait_send()
         for s in range(samples):
             rows_copy(s, step, me_tp).wait_send()
 
@@ -606,7 +645,7 @@
     n_sp, n_tp, n_dp = lax.axis_size("sp"), lax.axis_size("tp"), lax.axis_size("dp")
     q_cols = w_query.shape[1]
     heads = q_cols // HEAD
-    assert w_key.shape[1] == HEAD and tokens % GRID_COLS == 0 and samples < 4 and heads % 4 == 0
+    assert w_key.shape[1] == HEAD and tokens % GRID_COLS == 0 and samples < 4 and heads % 4 == 0 and n_tp == 4 and samples == 2
     part = w_shift.shape[1]
     block = tokens // n_tp
     ctx_all = n_sp * ctx_rows
@@ -620,7 +659,7 @@
     V = pltpu.VMEM
     return pl.pallas_call(
         functools.partial(kernel, (n_sp, n_tp, n_dp)),
-        out_shape=jax.ShapeDtypeStruct((samples, block, width), bf16),
+        out_shape=V((samples, block, width), bf16),
         in_specs=[anywhere] * 2 + [vmem] * 3 + [anywhere] * 7 + [smem] * 2,
         out_specs=vmem,
         scratch_shapes=[
@@ -673,13 +712,13 @@
             dma((samples, 2)),
             dma((samples, n_tp)),
             dma((samples, n_tp)),
-            dma((n_tp,)),
-            dma((n_tp,)),
-            dma((n_tp, n_dp)),
-            dma((n_tp, n_dp)),
+            dma((3, PIECES)),
+            dma((3, PIECES)),
+            dma((3, n_dp)),
+            dma((3, n_dp)),
         ],
         compiler_params=pltpu.CompilerParams(
-            collective_id=0, has_side_effects=True, vmem_limit_bytes=60 * 1024 * 1024
+            collective_id=0, has_side_effects=True, vmem_limit_bytes=56 * 1024 * 1024
         ),
     )(
         latent,

time: 56.8 us -> 47 us (0.83)
  Pallas kernels: 53.5 us -> 45.4 us
  local copies, waits for them, and re-layouts: 3.16 us -> 1.32 us
    pallas_call x1, Pallas kernels: 53.5 us -> 45.4 us  [shards(): pl.pallas_call(functools.partial(kernel, (n_sp, n_tp, n_dp)), out_shape=V...]
    unnamed x1, local copies, waits for them, and re-layouts: 3.16 us -> 1.32 us
where the time goes in v2:
time: 47 us; the launch traced here: 46.7 us
  Pallas kernels  45.4 us (97%)
  local copies, waits for them, and re-layouts  1.32 us (3%)
    pallas_call x1, Pallas kernels, shards(): pl.pallas_call(functools.partial(kernel, (n_sp, n_tp, n_dp)), out_shape=V...  45.4 us
    unnamed x1, local copies, waits for them, and re-layouts  1.32 us

profile of v2, /device:TPU:0, one launch (start us, length us, event | category | flops | bytes accessed | tf_op | source)
XLA Modules:
  0.0 46.7 jit_solution(11920143044637833213)
XLA Ops:
  0.0 45.4 %shard_map.136 = bf16[2,256,2048]{2,1,0:T(8,128)(2,1)S(1)} custom-call(bf16[2,1024,2048]{2,1,0:T(8,128)(2,1)} %latent.1, bf16[2,256,2048]{2,1,0:T(8,128)(2,1)} %context.1, bf16[2,512]{1,0:T(2,128)(2,1)} %condition.1, bf16[512]{0:T(512)(128)(2,1)} %ctx_cond.1, f32[1,2048]{1,0:T(1,128)} %bitcast.5, bf16[512,512]{1,0:T(8,128)(2,1)} %w_shift.1, ...), custom_call_target="tpu_custom_call" | custom-call | tf_op jit(solution)/shard_map/pallas_call | solution.py:660
  45.4 1.3 %copy.16 = bf16[2,256,2048]{2,1,0:T(8,128)(2,1)} copy(bf16[2,256,2048]{2,1,0:T(8,128)(2,1)S(1)} %shard_map.136) | data formatting | bytes 4194304

commit v3 on v2

--- a/solution.py
+++ b/solution.py
@@ -14,6 +14,7 @@
 LANES = 128
 ONES = 16
 PIECES = 4
+AHEAD = 2
 
 epsilon = 1e-06
 rope_base = 10000.0
@@ -29,9 +30,9 @@
     sizes,
     latent,
     context,
-    condition,
-    ctx_cond,
-    norm_gain,
+    condition_in,
+    ctx_cond_in,
+    norm_gain_in,
     w_shift,
     w_scale,
     w_gate,
@@ -39,9 +40,14 @@
     w_key,
     w_value,
     w_out,
+    sink_logit_in,
+    ctx_lift_in,
+    out,
+    condition,
+    ctx_cond,
+    norm_gain,
     sink_logit,
     ctx_lift,
-    out,
     x_lat,
     x_ctx,
     w_mod,
@@ -74,8 +80,11 @@
     mask_buf,
     s_a,
     s_b,
+    s_c,
+    s_d,
     att_buf,
     rows_rx,
+    mix_buf,
     ld_sem,
     ma_send,
     ma_recv,
@@ -120,6 +129,8 @@
 
     loads = []
     for source, target in (
+        (condition_in, condition),
+        (ctx_cond_in, ctx_cond),
         (w_shift, w_mod.at[0]),
         (w_scale, w_mod.at[1]),
         (context, x_ctx),
@@ -128,6 +139,9 @@
         (w_query, w_q),
         (w_gate, w_mod.at[2]),
         *((latent.at[s], x_lat.at[s]) for s in range(samples)),
+        (norm_gain_in, norm_gain),
+        (sink_logit_in, sink_logit),
+        (ctx_lift_in, ctx_lift),
         (w_out, w_o.at[me_tp]),
     ):
         copy = pltpu.make_async_copy(source, target, ld_sem.at[len(loads)])
@@ -211,13 +225,15 @@
         )
 
     act[...] = jnp.zeros_like(act)
+    loads[0].wait()
+    loads[1].wait()
     cond = condition[...].astype(f32)
     act[0:samples, :] = cond / (1.0 + jnp.exp(-cond))
     cond = ctx_cond[...].astype(f32).reshape(1, -1)
     act[samples : samples + 1, :] = cond / (1.0 + jnp.exp(-cond))
     active = act[...].astype(bf16)
     for i in range(2):
-        loads[i].wait()
+        loads[2 + i].wait()
         mod_rx[me_sp, :, i * part : (i + 1) * part] = jnp.dot(
             active, w_mod[i], preferred_element_type=f32
         )[0:keep_rows]
@@ -226,19 +242,19 @@
     own_copy(0, 0).start()
     own_copy(1, 0).start()
 
-    loads[6].wait()
+    loads[8].wait()
     gate_rx[me_sp] = jnp.dot(active, w_mod[2], preferred_element_type=f32)[0:keep_rows]
     gate_a[0]()
 
-    loads[2].wait()
+    loads[4].wait()
     for s in range(samples):
         wide = x_ctx[s].astype(f32)
         total = jnp.sum(wide * wide, axis=-1, keepdims=True)
         inv_ctx[s] = jnp.broadcast_to(lax.rsqrt(total / width + epsilon), (ctx_rows, LANES))
 
-    loads[3].wait()
-    loads[4].wait()
     loads[5].wait()
+    loads[6].wait()
+    loads[7].wait()
     for i in range(0, width, 256):
         w_t[0:q_cols, i : i + 256] = w_q[i : i + 256, :].T
 
@@ -265,7 +281,7 @@
 
         lax.fori_loop(0, n_tp, body, 0)
 
-    loads[7].wait()
+    loads[9].wait()
     stats(0)
 
     mod_a[1]()
@@ -279,7 +295,7 @@
         own_copy(1, i).start()
 
     for s in range(1, samples):
-        loads[7 + s].wait()
+        loads[9 + s].wait()
         stats(s)
 
     gate_a[1]()
@@ -288,6 +304,9 @@
         total = total + gate_rx[i]
     gate_all[me_tp] = total
     gate_b[0]()
+
+    for i in range(2, 5):
+        loads[-i].wait()
 
     mod_b[1]()
     for t in range(n_tp):
@@ -391,6 +410,8 @@
         if s < 2:
             relay(s * PIECES // 2, (s + 1) * PIECES // 2)
 
+    halves = block // LANES
+
     def rows_copy(s, step, source):
         target = other(me_tp, step, n_tp)
         return pltpu.make_async_remote_copy(
@@ -403,7 +424,6 @@
         )
 
     pairs = heads // 2
-    halves = block // LANES
     near_rows = LANES + 2 * WINDOW
     low = lax.broadcasted_iota(jnp.int32, (1, 2 * LANES), 1) < LANES
 
@@ -415,10 +435,13 @@
         owner = other(me_tp, step, n_tp)
         return pl.multiple_of(owner * block + (index % halves) * LANES, LANES)
 
-    chunks = [(False, 0, 2 * WINDOW), (False, 2 * WINDOW, LANES)]
-    far_chunk = min(256, ctx_all)
-    for c in range(0, ctx_all, far_chunk):
-        chunks.append((True, c, far_chunk))
+    def chunks_of(near, far):
+        return [(False, c, min(near, near_rows - c)) for c in range(0, near_rows, near)] + [
+            (True, c, min(far, ctx_all)) for c in range(0, ctx_all, min(far, ctx_all))
+        ]
+
+    score_chunks = chunks_of(384, 256)
+    value_chunks = chunks_of(256, 256)
 
     def score_steps(s, index, pair, buf, state):
         start = start_of(index)
@@ -437,18 +460,17 @@
             scores = jnp.dot(keys, q, preferred_element_type=f32)
             base = near_rows + first if far else first
             if not far:
-                mask = mask_buf[0 if first == 0 else 1]
-                mask = jnp.concatenate([mask, mask], axis=1)
-                edge = scores[0:WINDOW] + mask
-                if count > WINDOW:
-                    scores = jnp.concatenate([edge, scores[WINDOW:]], axis=0)
-                else:
-                    scores = edge
+                parts = [scores[r : r + WINDOW] for r in range(0, count, WINDOW)]
+                for edge, place in ((0, 0), (1, near_rows - WINDOW)):
+                    if first <= place < first + count:
+                        mask = jnp.concatenate([mask_buf[edge], mask_buf[edge]], axis=1)
+                        parts[(place - first) // WINDOW] += mask
+                scores = jnp.concatenate(parts, axis=0)
             buf[base : base + count, :] = scores
             high = jnp.max(scores.reshape(count // 8, 8, 2 * LANES), axis=0)
             tops[far] = high if tops[far] is None else jnp.maximum(tops[far], high)
 
-        for chunk in chunks:
+        for chunk in score_chunks:
             yield functools.partial(one, chunk)
 
         def close():
@@ -477,7 +499,7 @@
             term = jnp.dot(values, p, preferred_element_type=f32)
             acc[0] = term if acc[0] is None else acc[0] + term
 
-        for chunk in chunks:
+        for chunk in value_chunks:
             yield functools.partial(one, chunk)
 
         def close():
@@ -493,39 +515,44 @@
         yield close
 
     def run(*streams):
-        for steps in zip(*streams):
-            for step in steps:
-                step()
-
-    bufs = (s_a, s_b)
+        streams = [list(steps) for steps in streams]
+        order = sorted(
+            ((i + 1) / len(steps), k, i) for k, steps in enumerate(streams) for i in range(len(steps))
+        )
+        for _, k, i in order:
+            streams[k][i]()
+
+    bufs = (s_a, s_b, s_c, s_d)
+    per_step = halves * pairs
 
     def attention(s):
-        count = n_tp * halves
-        top0 = []
-        run(score_steps(s, 0, 0, s_a, top0))
-
-        def body(index, top, last):
-            for pair in range(pairs):
-                mine_buf, next_buf = bufs[pair % 2], bufs[(pair + 1) % 2]
-                fresh = []
-                streams = [value_steps(s, index, pair, mine_buf, top)]
-                if pair + 1 < pairs:
-                    streams.insert(0, score_steps(s, index, pair + 1, next_buf, fresh))
-                elif not last:
-                    streams.insert(0, score_steps(s, index + 1, 0, next_buf, fresh))
+        def scores_of(unit, base, target):
+            return score_steps(s, base + unit // pairs, unit % pairs, bufs[unit % len(bufs)], target)
+
+        tops = [[] for _ in range(AHEAD)]
+        run(*(scores_of(unit, 0, tops[unit]) for unit in range(AHEAD)))
+
+        def body(step, tops, last):
+            base = step * halves
+            known = [[top] for top in tops]
+            for unit in range(per_step):
+                streams = []
+                if not last or unit + AHEAD < per_step:
+                    known.append([])
+                    streams.append(scores_of(unit + AHEAD, base, known[-1]))
+                streams.append(
+                    value_steps(
+                        s, base + unit // pairs, unit % pairs, bufs[unit % len(bufs)], known[unit][0]
+                    )
+                )
                 run(*streams)
-                top = fresh[0] if fresh else top
-
-            step = index // halves + 1
-
-            @pl.when((index % halves == halves - 1) & (step < n_tp))
-            def _():
-                rows_copy(s, step, me_tp).start()
-
-            return top
-
-        top = lax.fori_loop(0, count - 1, lambda i, top: body(i, top, False), top0[0])
-        body(count - 1, top, True)
+            if not last:
+                rows_copy(s, step + 1, me_tp).start()
+            return tuple(top[0] for top in known[per_step:])
+
+        tops = tuple(top[0] for top in tops)
+        tops = lax.fori_loop(0, n_tp - 1, lambda step, tops: body(step, tops, False), tops)
+        body(n_tp - 1, tops, True)
         rows_rx[me_tp, s] = att_buf[s, me_tp]
 
     def context_ready(s):
@@ -567,19 +594,33 @@
         for hop in range(1, n_dp):
             forward_copy(source, index, hop, other(me_dp, n_dp - hop, n_dp)).wait_recv()
     chunk = 512
+
+    def rows_arrive(s, step):
+        rows_copy(s, step, other(me_tp, n_tp - step, n_tp)).wait_recv()
+
+    def mix(s, steps, c):
+        acc = None
+        for step in steps:
+            t = other(me_tp, n_tp - step, n_tp)
+            term = jnp.dot(rows_rx[t, s], w_o[t, :, c : c + chunk], preferred_element_type=f32)
+            acc = term if acc is None else acc + term
+        return acc
+
     for s in range(samples):
-        for step in range(1, n_tp):
-            rows_copy(s, step, other(me_tp, n_tp - step, n_tp)).wait_recv()
-
-        def finish(i, carry):
-            cols = pl.ds(pl.multiple_of(i * chunk, chunk), chunk)
-            acc = jnp.dot(rows_rx[0, s], w_o[0, :, cols], preferred_element_type=f32)
-            for t in range(1, n_tp):
-                acc += jnp.dot(rows_rx[t, s], w_o[t, :, cols], preferred_element_type=f32)
-            out[s, :, cols] = (acc * vec_g[s : s + 1, cols]).astype(bf16)
-            return carry
-
-        lax.fori_loop(0, width // chunk, finish, 0)
+        final = s == samples - 1
+        for step in range(1, n_tp - 1 if final else n_tp):
+            rows_arrive(s, step)
+        for c in range(0, width, chunk):
+            cols = slice(c, c + chunk)
+            if final:
+                mix_buf[:, cols] = mix(s, range(n_tp - 1), c)
+            else:
+                out[s, :, cols] = (mix(s, range(n_tp), c) * vec_g[s : s + 1, cols]).astype(bf16)
+    rows_arrive(samples - 1, n_tp - 1)
+    for c in range(0, width, chunk):
+        cols = slice(c, c + chunk)
+        acc = mix_buf[:, cols] + mix(samples - 1, (n_tp - 1,), c)
+        out[samples - 1, :, cols] = (acc * vec_g[samples - 1 : samples, cols]).astype(bf16)
 
     for _, _, finish_send in (mod_a, mod_b, gate_a, gate_b):
         finish_send()
@@ -650,7 +691,6 @@
     block = tokens // n_tp
     ctx_all = n_sp * ctx_rows
     vmem = pl.BlockSpec(memory_space=pltpu.VMEM)
-    smem = pl.BlockSpec(memory_space=pltpu.SMEM)
     anywhere = pl.BlockSpec(memory_space=pl.ANY)
     dma = pltpu.SemaphoreType.DMA
     padded = tokens + 2 * WINDOW
@@ -660,9 +700,14 @@
     return pl.pallas_call(
         functools.partial(kernel, (n_sp, n_tp, n_dp)),
         out_shape=V((samples, block, width), bf16),
-        in_specs=[anywhere] * 2 + [vmem] * 3 + [anywhere] * 7 + [smem] * 2,
+        in_specs=[anywhere] * 14,
         out_specs=vmem,
         scratch_shapes=[
+            V(condition.shape, bf16),
+            V(ctx_cond.shape, bf16),
+            V((1, width), f32),
+            pltpu.SMEM(sink_logit.shape, f32),
+            pltpu.SMEM(ctx_lift.shape, f32),
             V(latent.shape, bf16),
             V(context.shape, bf16),
             V((3,) + w_shift.shape, bf16),
@@ -695,9 +740,12 @@
             V((2, WINDOW, LANES), f32),
             V((keys, 2 * LANES), f32),
             V((keys, 2 * LANES), f32),
+            V((keys, 2 * LANES), f32),
+            V((keys, 2 * LANES), f32),
             V((samples, n_tp, block, q_cols), bf16),
             V((n_tp, samples, block, q_cols), bf16),
-            dma((8 + samples,)),
+            V((block, width), f32),
+            dma((13 + samples,)),
             dma((n_sp,)),
             dma((n_sp,)),
             dma((n_tp,)),

time: 47 us -> 41.1 us (0.87)
  Pallas kernels: 45.4 us -> 39.6 us
    pallas_call x1, Pallas kernels: 45.4 us -> 39.6 us  [shards(): pl.pallas_call(functools.partial(kernel, (n_sp, n_tp, n_dp)), out_shape=V...]
where the time goes in v3:
time: 41.1 us; the launch traced here: 40.9 us
  Pallas kernels  39.6 us (96%)
  local copies, waits for them, and re-layouts  1.32 us (3%)
    pallas_call x1, Pallas kernels, shards(): pl.pallas_call(functools.partial(kernel, (n_sp, n_tp, n_dp)), out_shape=V...  39.6 us
    unnamed x1, local copies, waits for them, and re-layouts  1.32 us

profile of v3, /device:TPU:0, one launch (start us, length us, event | category | flops | bytes accessed | tf_op | source)
XLA Modules:
  0.0 40.9 jit_solution(6333895461479885186)
XLA Ops:
  0.0 39.6 %shard_map.136 = bf16[2,256,2048]{2,1,0:T(8,128)(2,1)S(1)} custom-call(bf16[2,1024,2048]{2,1,0:T(8,128)(2,1)} %latent.1, bf16[2,256,2048]{2,1,0:T(8,128)(2,1)} %context.1, bf16[2,512]{1,0:T(2,128)(2,1)} %condition_in.1, bf16[512]{0:T(512)(128)(2,1)} %ctx_cond_in.1, f32[1,2048]{1,0:T(1,128)} %bitcast.5, bf16[512,512]{1,0:T(8,128)(2,1)} %w_shift.1, ...), custom_call_target="tpu_custom_call" | custom-call | tf_op jit(solution)/shard_map/pallas_call | solution.py:700
  39.6 1.3 %copy.16 = bf16[2,256,2048]{2,1,0:T(8,128)(2,1)} copy(bf16[2,256,2048]{2,1,0:T(8,128)(2,1)S(1)} %shard_map.136) | data formatting | bytes 4194304

commit v4 on v3

--- a/solution.py
+++ b/solution.py
@@ -13,7 +13,8 @@
 GRID_COLS = 64
 LANES = 128
 ONES = 16
-PIECES = 4
+PIECES = 8
+EARLY = 2
 AHEAD = 2
 
 epsilon = 1e-06
@@ -196,6 +197,13 @@
             device_id_type=MESH,
         )
 
+    own_order = (range(PIECES), [(i + PIECES // 2) % PIECES for i in range(PIECES)])
+
+    def own_start(first, last):
+        for i in range(first, last):
+            for kind in range(2):
+                own_copy(kind, own_order[kind][i]).start()
+
     def own_copy(kind, i):
         return piece_copy(kind, i, me_tp, (across, along)[kind], w_out)
 
@@ -208,10 +216,11 @@
         target = (across, along, (along, across)[2 * i // PIECES])[kind]
         piece_copy(kind, i, source, target, w_o.at[source]).wait_recv()
 
-    def relay(first, last):
-        for i in range(first, last):
-            piece_arrive(2 * i // PIECES, i)
-            relay_copy(i).start()
+    def relay():
+        for i in range(PIECES // 2):
+            for kind in range(2):
+                piece_arrive(kind, own_order[kind][i])
+                relay_copy(own_order[kind][i]).start()
 
     def forward_copy(source, index, hop, part_id):
         rows = pl.ds(pl.multiple_of(part_id * share, share), share)
@@ -236,11 +245,10 @@
         loads[2 + i].wait()
         mod_rx[me_sp, :, i * part : (i + 1) * part] = jnp.dot(
             active, w_mod[i], preferred_element_type=f32
-        )[0:keep_rows]
+        )[0:keep_rows].astype(bf16)
     pl.semaphore_wait(barrier, n_sp + n_tp + n_dp - 3)
     mod_a[0]()
-    own_copy(0, 0).start()
-    own_copy(1, 0).start()
+    own_start(0, EARLY)
 
     loads[8].wait()
     gate_rx[me_sp] = jnp.dot(active, w_mod[2], preferred_element_type=f32)[0:keep_rows]
@@ -285,14 +293,12 @@
     stats(0)
 
     mod_a[1]()
-    total = mod_rx[0]
+    total = mod_rx[0].astype(f32)
     for i in range(1, n_sp):
-        total = total + mod_rx[i]
-    mod_all[me_tp] = total
+        total = total + mod_rx[i].astype(f32)
+    mod_all[me_tp] = total.astype(bf16)
     mod_b[0]()
-    for i in range(1, PIECES):
-        own_copy(0, i).start()
-        own_copy(1, i).start()
+    own_start(EARLY, PIECES)
 
     for s in range(1, samples):
         loads[9 + s].wait()
@@ -311,8 +317,8 @@
     mod_b[1]()
     for t in range(n_tp):
         cols = slice(t * part, (t + 1) * part)
-        vec_b[0:keep_rows, cols] = mod_all[t, :, 0:part]
-        vec_a[0:keep_rows, cols] = (1.0 + mod_all[t, :, part : 2 * part]) * norm_gain[:, cols]
+        vec_b[0:keep_rows, cols] = mod_all[t, :, 0:part].astype(f32)
+        vec_a[0:keep_rows, cols] = (1.0 + mod_all[t, :, part : 2 * part].astype(f32)) * norm_gain[:, cols]
 
     def fold(target, first, last, base, row):
         gain = vec_a[row : row + 1, :]
@@ -341,8 +347,15 @@
         rows = pl.ds(pl.multiple_of(me_sp * ctx_rows, ctx_rows), ctx_rows)
         kv = lax.dot_general(x_ctx[s], w_c[...], nt, preferred_element_type=f32)
         ckv_buf[s, rows, :] = (kv * inv_ctx[s] + bias_row[samples : samples + 1, :]).astype(bf16)
-        for step in range(1, n_sp):
-            ctx_copy(s, step, me_sp).start()
+        for far in range(n_sp - 1, 0, -1):
+
+            @pl.when(me_sp + far < n_sp)
+            def _():
+                ctx_copy(s, far, me_sp).start()
+
+            @pl.when(me_sp >= far)
+            def _():
+                ctx_copy(s, n_sp - far, me_sp).start()
 
     context_keys(0)
 
@@ -367,6 +380,15 @@
             device_id={"sp": other(me_sp, step, n_sp)},
             device_id_type=MESH,
         )
+
+    has_left, has_right = me_sp > 0, me_sp < n_sp - 1
+
+    def halo_sends(s, act_on):
+        for side, present in ((0, has_right), (1, has_left)):
+
+            @pl.when(present)
+            def _():
+                act_on(halo_copy(s, side))
 
     def project(s, start):
         cols = slice(start, start + block)
@@ -400,15 +422,16 @@
         kv_buf[s, WINDOW + start : WINDOW + start + block, :] = kv.T.astype(bf16)
 
     for s in range(samples):
+        fold_sample(s)
+        project(s, 0)
+        project(s, tokens - block)
+        halo_sends(s, lambda copy: copy.start())
+        for i in range(1, n_tp - 1):
+            project(s, i * block)
         if s > 0:
             context_keys(s)
-        fold_sample(s)
-        for i in range(n_tp):
-            project(s, i * block)
-        halo_copy(s, 0).start()
-        halo_copy(s, 1).start()
-        if s < 2:
-            relay(s * PIECES // 2, (s + 1) * PIECES // 2)
+        if s == 0:
+            relay()
 
     halves = block // LANES
 
@@ -525,6 +548,15 @@
     bufs = (s_a, s_b, s_c, s_d)
     per_step = halves * pairs
 
+    def forward(kinds):
+        for index in kinds:
+            source = (across, along, diagonal)[index]
+            for i in range(PIECES):
+                if index == 2 or 2 * i // PIECES != index:
+                    piece_arrive(index, i)
+            for hop in range(1, n_dp):
+                forward_copy(source, index, hop, me_dp).start()
+
     def attention(s):
         def scores_of(unit, base, target):
             return score_steps(s, base + unit // pairs, unit % pairs, bufs[unit % len(bufs)], target)
@@ -548,6 +580,8 @@
                 run(*streams)
             if not last:
                 rows_copy(s, step + 1, me_tp).start()
+                if s == samples - 1:
+                    pl.when(step == 0)(lambda: forward((2,)))
             return tuple(top[0] for top in known[per_step:])
 
         tops = tuple(top[0] for top in tops)
@@ -563,27 +597,27 @@
 
     def halo_ready(s):
         for side in range(2):
-            halo_copy(s, side).wait_recv()
             first = (0, WINDOW + tokens)[side]
-            valid = (me_sp > 0, me_sp < n_sp - 1)[side]
-            rows = jnp.where(valid, kv_buf[s, first : first + WINDOW, :].astype(f32), 0.0)
-            kv_buf[s, first : first + WINDOW, :] = rows.astype(bf16)
-            vt_buf[s, 0:HEAD, first : first + WINDOW] = rows.T[HEAD:].astype(bf16)
-            vt_buf[s, HEAD:, first : first + WINDOW] = jnp.where(
-                valid, jnp.ones((ONES, WINDOW), f32), 0.0
-            ).astype(bf16)
+            valid = (has_left, has_right)[side]
+            halo = slice(first, first + WINDOW)
+
+            @pl.when(valid)
+            def _():
+                halo_copy(s, side).wait_recv()
+
+            @pl.when(jnp.logical_not(valid))
+            def _():
+                kv_buf[s, halo, :] = jnp.zeros((WINDOW, LANES), bf16)
+                vt_buf[s, HEAD:, halo] = jnp.zeros((ONES, WINDOW), bf16)
+
+            vt_buf[s, 0:HEAD, halo] = kv_buf[s, halo, :].T[HEAD:]
 
     for s in range(samples):
         halo_ready(s)
         context_ready(s)
         attention(s)
         if s == 0:
-            for index, source in enumerate((across, along, diagonal)):
-                for i in range(PIECES):
-                    if index == 2 or 2 * i // PIECES != index:
-                        piece_arrive(index, i)
-                for hop in range(1, n_dp):
-                    forward_copy(source, index, hop, me_dp).start()
+            forward((0, 1))
 
     gate_b[1]()
     for t in range(n_tp):
@@ -627,8 +661,7 @@
     for s in range(samples):
         for step in range(1, n_sp):
             ctx_copy(s, step, me_sp).wait_send()
-        halo_copy(s, 0).wait_send()
-        halo_copy(s, 1).wait_send()
+        halo_sends(s, lambda copy: copy.wait_send())
     for i in range(PIECES):
         own_copy(0, i).wait_send()
         own_copy(1, i).wait_send()
@@ -721,8 +754,8 @@
             V((HEAD // 4, block), f32),
             V((n_tp,) + w_out.shape, bf16),
             V((8, w_shift.shape[0]), f32),
-            V((n_sp, 4, 2 * part), f32),
-            V((n_tp, 4, 2 * part), f32),
+            V((n_sp, 4, 2 * part), bf16),
+            V((n_tp, 4, 2 * part), bf16),
             V((n_sp, 4, part), f32),
             V((n_tp, 4, part), f32),
             V((8, width), f32),

time: 41.1 us -> 40.2 us (0.978)
  Pallas kernels: 39.6 us -> 38.7 us
    pallas_call x1, Pallas kernels: 39.6 us -> 38.7 us  [shards(): pl.pallas_call(functools.partial(kernel, (n_sp, n_tp, n_dp)), out_shape=V...]
where the time goes in v4:
time: 40.2 us; the launch traced here: 40.1 us
  Pallas kernels  38.7 us (96%)
  local copies, waits for them, and re-layouts  1.32 us (3%)
    pallas_call x1, Pallas kernels, shards(): pl.pallas_call(functools.partial(kernel, (n_sp, n_tp, n_dp)), out_shape=V...  38.7 us
    unnamed x1, local copies, waits for them, and re-layouts  1.32 us

profile of v4, /device:TPU:0, one launch (start us, length us, event | category | flops | bytes accessed | tf_op | source)
XLA Modules:
  0.0 40.1 jit_solution(11908065578693464376)
XLA Ops:
  0.0 38.7 %shard_map.136 = bf16[2,256,2048]{2,1,0:T(8,128)(2,1)S(1)} custom-call(bf16[2,1024,2048]{2,1,0:T(8,128)(2,1)} %latent.1, bf16[2,256,2048]{2,1,0:T(8,128)(2,1)} %context.1, bf16[2,512]{1,0:T(2,128)(2,1)} %condition_in.1, bf16[512]{0:T(512)(128)(2,1)} %ctx_cond_in.1, f32[1,2048]{1,0:T(1,128)} %bitcast.5, bf16[512,512]{1,0:T(8,128)(2,1)} %w_shift.1, ...), custom_call_target="tpu_custom_call" | custom-call | tf_op jit(solution)/shard_map/pallas_call | solution.py:733
  38.7 1.3 %copy.16 = bf16[2,256,2048]{2,1,0:T(8,128)(2,1)} copy(bf16[2,256,2048]{2,1,0:T(8,128)(2,1)S(1)} %shard_map.136) | data formatting | bytes 4194304

commit v5 on v4

--- a/solution.py
+++ b/solution.py
@@ -347,17 +347,21 @@
         rows = pl.ds(pl.multiple_of(me_sp * ctx_rows, ctx_rows), ctx_rows)
         kv = lax.dot_general(x_ctx[s], w_c[...], nt, preferred_element_type=f32)
         ckv_buf[s, rows, :] = (kv * inv_ctx[s] + bias_row[samples : samples + 1, :]).astype(bf16)
+
+    def context_sends(s, turn):
         for far in range(n_sp - 1, 0, -1):
 
-            @pl.when(me_sp + far < n_sp)
+            @pl.when(turn & (me_sp + far < n_sp))
             def _():
                 ctx_copy(s, far, me_sp).start()
 
-            @pl.when(me_sp >= far)
+            @pl.when(turn & (me_sp >= far))
             def _():
                 ctx_copy(s, n_sp - far, me_sp).start()
 
+    first_turn = me_dp < n_dp - 1
     context_keys(0)
+    context_sends(0, me_sp >= 0)
 
     def fold_sample(s):
         fold(w_s.at[s], 0, q_cols + 2 * HEAD, 0, s)
@@ -430,13 +434,20 @@
             project(s, i * block)
         if s > 0:
             context_keys(s)
+            context_sends(s, first_turn)
         if s == 0:
             relay()
 
     halves = block // LANES
 
+    to_across = 1 - 2 * lax.rem(me_tp, 2)
+    to_along = 2 - 4 * lax.div(me_tp, 2)
+
+    def partner(step):
+        return me_tp + to_across * ((4 - step) // 2) + to_along * (step % 2)
+
     def rows_copy(s, step, source):
-        target = other(me_tp, step, n_tp)
+        target = partner(step)
         return pltpu.make_async_remote_copy(
             src_ref=att_buf.at[s, target],
             dst_ref=rows_rx.at[source, s],
@@ -454,8 +465,7 @@
         return jnp.where(low, ref[2 * pair], ref[2 * pair + 1]) * log2e
 
     def start_of(index):
-        step = index // halves + 1
-        owner = other(me_tp, step, n_tp)
+        owner = partner(index // halves + 1)
         return pl.multiple_of(owner * block + (index % halves) * LANES, LANES)
 
     def chunks_of(near, far):
@@ -529,7 +539,7 @@
             weight = acc[0][HEAD : HEAD + 1] + jnp.exp2(two(sink_logit, pair) - top)
             rows = acc[0][0:HEAD] * (1.0 / weight)
             stacked = jnp.concatenate([rows[:, 0:LANES], rows[:, LANES:]], axis=0)
-            owner = other(me_tp, index // halves + 1, n_tp)
+            owner = partner(index // halves + 1)
             half = pl.multiple_of((index % halves) * LANES, LANES)
             att_buf[s, owner, pl.ds(half, LANES), pair * LANES : (pair + 1) * LANES] = (
                 stacked.T.astype(bf16)
@@ -615,6 +625,8 @@
     for s in range(samples):
         halo_ready(s)
         context_ready(s)
+        if s + 1 < samples:
+            context_sends(s + 1, jnp.logical_not(first_turn))
         attention(s)
         if s == 0:
             forward((0, 1))
@@ -630,12 +642,12 @@
     chunk = 512
 
     def rows_arrive(s, step):
-        rows_copy(s, step, other(me_tp, n_tp - step, n_tp)).wait_recv()
+        rows_copy(s, step, partner(step)).wait_recv()
 
     def mix(s, steps, c):
         acc = None
         for step in steps:
-            t = other(me_tp, n_tp - step, n_tp)
+            t = partner(step) if step else me_tp
             term = jnp.dot(rows_rx[t, s], w_o[t, :, c : c + chunk], preferred_element_type=f32)
             acc = term if acc is None else acc + term
         return acc

time: 40.2 us -> 40.2 us (level)
  no operation moved by 1% of the time
where the time goes in v5:
time: 40.2 us; the launch traced here: 40 us
  Pallas kernels  38.7 us (96%)
  local copies, waits for them, and re-layouts  1.32 us (3%)
    pallas_call x1, Pallas kernels, shards(): pl.pallas_call(functools.partial(kernel, (n_sp, n_tp, n_dp)), out_shape=V...  38.7 us
    unnamed x1, local copies, waits for them, and re-layouts  1.32 us

profile of v5, /device:TPU:0, one launch (start us, length us, event | category | flops | bytes accessed | tf_op | source)
XLA Modules:
  0.0 40.0 jit_solution(16819077193626202574)
XLA Ops:
  0.0 38.7 %shard_map.136 = bf16[2,256,2048]{2,1,0:T(8,128)(2,1)S(1)} custom-call(bf16[2,1024,2048]{2,1,0:T(8,128)(2,1)} %latent.1, bf16[2,256,2048]{2,1,0:T(8,128)(2,1)} %context.1, bf16[2,512]{1,0:T(2,128)(2,1)} %condition_in.1, bf16[512]{0:T(512)(128)(2,1)} %ctx_cond_in.1, f32[1,2048]{1,0:T(1,128)} %bitcast.5, bf16[512,512]{1,0:T(8,128)(2,1)} %w_shift.1, ...), custom_call_target="tpu_custom_call" | custom-call | tf_op jit(solution)/shard_map/pallas_call | solution.py:745
  38.7 1.3 %copy.16 = bf16[2,256,2048]{2,1,0:T(8,128)(2,1)} copy(bf16[2,256,2048]{2,1,0:T(8,128)(2,1)S(1)} %shard_map.136) | data formatting | bytes 4194304
